TPU v7x, 128 devices: a whole 4x4x4 slice. The times are simulated.
128 devices in a mesh: sp: 32 (over z, y, core), tp: 4 (over x).
Axes of the slice: x: 4, y: 4, z: 4, core: 2. Of those that a mesh axis runs over, the one named last changes fastest.
Arguments:
- tokens: bfloat16 [8192, 1024], P(('sp', 'tp')), may hold values from -7.5 to 7.5, as said below
- query_weight: bfloat16 [1024, 2048], P('sp', 'tp'), may hold values from -0.1875 to 0.1875
- key_weight: bfloat16 [1024, 2048], P('sp', 'tp'), may hold values from -0.1875 to 0.1875
- value_weight: bfloat16 [1024, 2048], P('sp', 'tp'), may hold values from -0.1875 to 0.1875
- gate_weight: bfloat16 [1024, 16], P('sp', 'tp'), may hold values from -0.1875 to 0.1875
- forget_bias: float32 [16], P('tp'), may hold values from 0 to 2
- out_weight: bfloat16 [2048, 1024], P('tp', 'sp'), may hold values from -0.125 to 0.125
- out_gain: float32 [1024], replicated, may hold values from 0.5 to 1.5
Outputs:
- mixed: bfloat16 [8192, 1024], P(('sp', 'tp'))
Inputs may be any that keep to these rules, and one draw needn't show every extreme that they name: `tokens`: each entry is a bounded noise value (at most 6 in size) plus an offset in -1.5 to 1.5 shared by the 256 rows of one index of sp, so every entry lies within -7.5 and 7.5.
All inputs are finite; a program needn't handle non-finite values.
Results may differ from a plain program's by a relative error of at most 0.006.
Values may be sent and summed in bfloat16 or wider, within the bound.
A program may use at most 128 MiB of HBM per device.

v0:
```python
import math

import jax
import jax.numpy as jnp
from jax import lax
from jax.sharding import Mesh
from jax.sharding import PartitionSpec as P

SP = ("sp_0", "sp_1", "sp_2")
SP_TP = ("sp_0", "sp_1", "sp_2", "tp")


def in_order(blocks, dim):
    shape = list(blocks.shape[1:])
    shape[dim] *= blocks.shape[0]
    return jnp.moveaxis(blocks, 0, dim).reshape(shape)


def one_gather(arrays, axis, dims):
    ravelled = jnp.concatenate([a.reshape(-1) for a in arrays])
    lines, at, done = lax.all_gather(ravelled, axis), 0, []
    for a, dim in zip(arrays, dims):
        blocks = lines[:, at : at + a.size].reshape(-1, *a.shape)
        done.append(in_order(blocks, dim))
        at += a.size
    return tuple(done)


def on_whole(shard, axis, dim, block):
    whole = lax.all_gather(shard, axis, axis=dim, tiled=True)
    return block(whole, jnp.int32(0))


def taken_in(shard, axis, dim, absorb, state):
    everything = jax.tree.map(lambda a: lax.all_gather(a, axis, axis=dim, tiled=True), shard)
    return absorb(state, everything, jnp.int32(0))


def all_blocks(shard, axes, order):
    blocks = shard[None]
    for k in order:
        blocks = lax.all_gather(blocks, axes[k], axis=0, tiled=True)
    carried = [lax.axis_size(axes[k]) for k in reversed(order)]
    blocks = blocks.reshape(*carried, *shard.shape)
    turned = sorted(range(len(order)), key=lambda place: order[len(order) - 1 - place])
    return blocks.transpose(*turned, *range(len(order), blocks.ndim)).reshape(-1, *shard.shape)


def gathered_by_axis(shard, axes, order, dim):
    return in_order(all_blocks(shard, axes, order), dim)


def summed_rows(product, width, axis):
    whole = product(jnp.int32(0), width * lax.axis_size(axis))
    return lax.psum_scatter(whole, axis, scatter_dimension=0, tiled=True)


def local(
    tokens, query_weight, key_weight, value_weight, gate_weight, forget_bias, out_weight, out_gain
):
    width = query_weight.shape[1]
    heads = gate_weight.shape[1]
    head_size = width // heads
    whole_q, whole_k, whole_v, whole_g = one_gather(
        (query_weight, key_weight, value_weight, gate_weight), SP, (0, 0, 0, 0)
    )
    joined = jnp.concatenate([whole_q, whole_k, whole_v, whole_g], axis=1)

    def project(piece, start):
        return jnp.dot(piece, joined, preferred_element_type=jnp.float32)

    projected = on_whole(tokens, "tp", 0, project)
    block = projected.shape[0]
    queries = projected[:, :width].astype(jnp.bfloat16).reshape(block, heads, head_size)
    keys = projected[:, width : 2 * width].astype(jnp.bfloat16).reshape(block, heads, head_size)
    values = (
        projected[:, 2 * width : 3 * width].astype(jnp.bfloat16).reshape(block, heads, head_size)
    )
    seq_len = block * lax.axis_size(SP)
    log_gate = jax.nn.log_sigmoid(projected[:, 3 * width :] + forget_bias + math.log(seq_len))
    gates_all = lax.all_gather(log_gate, SP, axis=0, tiled=True)
    cumulative = jnp.cumsum(gates_all, axis=0)
    first = lax.axis_index(SP) * block
    query_cum = lax.dynamic_slice_in_dim(cumulative, first, block, 0)
    query_pos = first + jnp.arange(block, dtype=jnp.int32)
    scale = head_size ** (-0.5)

    def update(carry, piece, start):
        run_max, run_sum, run_acc = carry
        key_piece, value_piece = piece
        length = key_piece.shape[0]
        key_cum = lax.dynamic_slice_in_dim(cumulative, start, length, 0)
        logits = (
            jnp.einsum("qhd,khd->hqk", queries, key_piece, preferred_element_type=jnp.float32)
            * scale
        )
        logits = logits + query_cum.T[:, :, None] - key_cum.T[:, None, :]
        key_pos = start + jnp.arange(length, dtype=jnp.int32)
        allowed = (key_pos[None, :] <= query_pos[:, None])[None]
        logits = jnp.where(allowed, logits, -1e30)
        new_max = jnp.maximum(run_max, jnp.max(logits, axis=-1))
        probs = jnp.where(allowed, jnp.exp(logits - new_max[..., None]), 0.0)
        factor = jnp.exp(run_max - new_max)
        new_sum = run_sum * factor + jnp.sum(probs, axis=-1)
        new_acc = run_acc * factor[..., None] + jnp.einsum(
            "hqk,khd->hqd", probs, value_piece.astype(jnp.float32)
        )
        return (new_max, new_sum, new_acc)

    def attend(carry, piece, start):
        return update(carry, piece, start)

    initial = (
        jnp.full((heads, block), -1e30, jnp.float32),
        jnp.zeros((heads, block), jnp.float32),
        jnp.zeros((heads, block, head_size), jnp.float32),
    )
    run_max, run_sum, run_acc = taken_in((keys, values), SP, 0, attend, initial)
    attended = (
        (run_acc / run_sum[..., None]).transpose(1, 0, 2).reshape(block, width).astype(jnp.bfloat16)
    )
    out_full = gathered_by_axis(out_weight, (("sp_0", "sp_1"), "sp_2"), (0, 1), 1)
    rows = tokens.shape[0]

    def term(start, count):
        return jnp.dot(
            lax.dynamic_slice_in_dim(attended, start, count, 0),
            out_full,
            preferred_element_type=jnp.float32,
        )

    summed = summed_rows(term, rows, "tp")
    normed = summed * lax.rsqrt(jnp.mean(summed * summed, axis=-1, keepdims=True) + 1e-06)
    return (normed * out_gain).astype(jnp.bfloat16)


def solution(mesh):
    torus = Mesh(mesh.devices.reshape(4, 4, 2, mesh.shape["tp"]), ("sp_0", "sp_1", "sp_2", "tp"))
    in_specs = (
        P(SP_TP, None),
        P(SP, "tp"),
        P(SP, "tp"),
        P(SP, "tp"),
        P(SP, "tp"),
        P("tp"),
        P("tp", SP),
        P(),
    )
    out_specs = P(SP_TP, None)
    return jax.shard_map(local, mesh=torus, in_specs=in_specs, out_specs=out_specs, check_vma=False)
```

profile of v0, /device:TPU:1, one launch (start us, length us, event | category | flops | bytes accessed | tf_op | source)
XLA Modules:
  0.0 242.4 jit_solution(11250575676439934487)
XLA Ops:
  6.5 0.0 copy-start.1
  6.5 0.0 all-gather.14.cloned.1.call-start
  6.5 0.8 copy.32
  7.3 0.8 copy.33
  8.1 0.8 copy.34
  8.9 0.8 copy.24
  9.7 0.1 reshape.93
  9.8 0.8 reshape.104
  10.6 0.0 all-gather.14.cloned.1.call-update
  10.6 0.0 all-gather.12.cloned.1.call-start
  10.6 21.8 %all-gather.1 = bf16[8192,32]{0,1:T(8,128)(2,1)S(1)} all-gather(bf16[512,32]{0,1:T(8,128)(2,1)} %param.14), channel_id=3, replica_groups=mesh['sp_0'=4,'sp_1'=4,'sp_2'=2,'tp'=4] {'sp_0','sp_1'}, dimensions={0}, use_global_device_ids=true | all-gather | bytes 557056 | tf_op jit(solution)/shard_map/all_gather | solution.py:42
  32.4 0.9 copy.37
  33.4 0.0 all-gather.12.cloned.1.call-update
  33.4 0.0 all-gather.8.cloned.1.call-start
  33.4 13.4 %all_gather.26 = bf16[256,1024]{1,0:T(8,128)(2,1)} all-gather(bf16[64,1024]{1,0:T(8,128)(2,1)} %param.8), channel_id=1, replica_groups=mesh['sp_0'=4,'sp_1'=4,'sp_2'=2,'tp'=4] {'tp'}, dimensions={0}, use_global_device_ids=true | all-gather | bytes 655360 | tf_op jit(solution)/shard_map/all_gather | solution.py:30
  46.8 17.4 %all-gather.14.cloned.1.call-done = bf16[32,1,49280]{2,1,0:T(2,128)(2,1)} async-done(((bf16[1,1,49280]{2,1,0:T(2,128)(2,1)}), bf16[32,1,49280]{2,1,0:T(2,128)(2,1)}) %all-gather.14.cloned.1.call-update) | async-done | bytes 3153936 | tf_op jit(solution)/shard_map/all_gather | solution.py:21
  64.2 3.1 %copy.41 = bf16[32,1,49280]{2,0,1:T(8,128)(2,1)S(1)} copy(bf16[32,1,49280]{2,1,0:T(2,128)(2,1)} %all-gather.14.cloned.1.call-done) | data formatting | bytes 6307840
  67.4 0.3 fusion.32
  67.7 1.3 reshape_reshape.12
  69.0 0.5 reshape_reshape.13
  69.5 0.5 reshape_reshape.14
  70.0 0.6 reshape_reshape.15
  70.6 3.6 %fusion.34 = (bf16[256,1540]{0,1:T(8,128)(2,1)S(1)}, f32[256,1540]{0,1:T(8,128)}) fusion(bf16[256,1024]{1,0:T(8,128)(2,1)} %all_gather.26, bf16[1024,4]{1,0:T(8,128)(2,1)S(1)} %reshape_reshape.15, bf16[1024,512]{1,0:T(8,128)(2,1)S(1)} %reshape_reshape.14, bf16[1024,512]{1,0:T(8,128)(2,1)S(1)} %reshape_reshape.13, bf16[1024,512]{1,0:T(8,128)(2,1)} %reshape_reshape.12), kind=kOutput, calls=%fused_computation.51 | convolution fusion | flops 820413440 | bytes 6043648 | tf_op jit(solution)/shard_map/dot_general | solution.py:70
  74.2 0.9 fusion.33
  75.1 0.8 copy.25
  75.9 0.0 all-gather.8.cloned.1.call-update
  75.9 0.0 all-gather.10.cloned.1.call-start
  76.0 0.5 all-gather.10.cloned.1.call-update
  76.5 0.0 reduce-scatter.2.cloned.1.call-start
  76.6 1.3 iota_compare_fusion
  77.8 0.0 all-gather.12.cloned.1.call-done
  77.9 1.8 copy.28
  79.7 0.0 copy-done.1
  79.7 0.8 fusion.25
  80.5 23.6 %all_gather.28 = f32[8192,4]{0,1:T(4,128)S(1)} all-gather(f32[256,4]{0,1:T(4,128)S(1)} %fusion.25), channel_id=1, replica_groups=mesh['sp_0'=4,'sp_1'=4,'sp_2'=2,'tp'=4] {'sp_0','sp_1','sp_2'}, dimensions={0}, use_global_device_ids=true | all-gather | bytes 135168 | tf_op jit(solution)/shard_map/all_gather | solution.py:81
  104.1 1.2 reduce-window.6
  105.3 0.2 slice_reduce_fusion
  105.5 0.2 reduce-window.9
  105.7 0.1 add_bitcast_fusion
  105.9 0.1 copy.42
  106.0 26.8 %all-gather.8.cloned.1.call-done = bf16[8192,4,128]{2,0,1:T(8,128)(2,1)} async-done(((bf16[256,4,128]{2,0,1:T(8,128)(2,1)}), bf16[8192,4,128]{2,0,1:T(8,128)(2,1)}) %all-gather.8.cloned.1.call-update) | async-done | bytes 8388624 | tf_op jit(solution)/shard_map/all_gather | solution.py:35
  132.8 19.3 %fusion.2 = (f32[4,256]{1,0:T(4,128)S(1)}, f32[4,256,8192]{2,1,0:T(8,128)}) fusion(f32[4,8192]{1,0:T(4,128)S(1)} %bitcast.67, f32[4,256]{1,0:T(4,128)S(1)} %constant_dynamic-slice_fusion, pred[256,8192]{1,0:T(8,128)(4,1)S(1)} %iota_compare_fusion, bf16[256,4,128]{0,2,1:T(8,128)(2,1)} %bitcast.73, bf16[8192,4,128]{2,0,1:T(8,128)(2,1)} %all-gather.8.cloned.1.call-done), kind=kOutput, calls=%fused_computation.4 | convolution fusion | flops 2189425664 | bytes 44441600 | tf_op jit(solution)/shard_map/qhd,khd->hqk/dot_general | solution.py:94
  152.1 17.7 %fusion = f32[4,256]{1,0:T(4,128)S(1)} fusion(f32[4,256,8192]{2,1,0:T(8,128)} %get-tuple-element.16, f32[4,256]{1,0:T(4,128)S(1)} %get-tuple-element.12, f32[4,8192]{1,0:T(4,128)S(1)} %bitcast.68, f32[4,256]{1,0:T(4,128)S(1)} %constant_dynamic-slice_fusion, pred[256,8192]{1,0:T(8,128)(4,1)S(1)} %iota_compare_fusion), kind=kLoop, calls=%fused_computation.2 | loop fusion | flops 58719232 | bytes 35794944 | tf_op jit(solution)/shard_map/reduce_sum | solution.py:104
  169.9 22.7 %all-gather.10.cloned.1.call-done = bf16[8192,4,128]{0,2,1:T(8,128)(2,1)} async-done(((bf16[256,4,128]{0,2,1:T(8,128)(2,1)}), bf16[8192,4,128]{0,2,1:T(8,128)(2,1)}) %all-gather.10.cloned.1.call-update) | async-done | bytes 8388624 | tf_op jit(solution)/shard_map/all_gather | solution.py:35
  192.6 0.0 copy-start
  192.6 17.6 %fusion.24 = bf16[256,4,128]{0,2,1:T(8,128)(2,1)S(1)} fusion(bf16[8192,4,128]{0,2,1:T(8,128)(2,1)} %all-gather.10.cloned.1.call-done, f32[4,256,8192]{2,1,0:T(8,128)} %get-tuple-element.16, f32[4,256]{1,0:T(4,128)S(1)} %get-tuple-element.12, f32[4,8192]{1,0:T(4,128)S(1)} %bitcast.69, f32[4,256]{1,0:T(4,128)S(1)} %constant_dynamic-slice_fusion, ...), kind=kOutput, calls=%fused_computation.26 | convolution fusion | flops 2198208512 | bytes 44449792 | tf_op jit(solution)/shard_map/hqk,khd->hqd/dot_general | solution.py:105
  210.2 1.5 fusion.35
  211.7 0.0 reduce-scatter.2.cloned.1.call-update
  211.7 21.3 %reduce-scatter.2.cloned.1.call-done = f32[64,1024]{1,0:T(8,128)} async-done(((f32[256,1024]{1,0:T(8,128)}), f32[64,1024]{1,0:T(8,128)}) %reduce-scatter.2.cloned.1.call-update) | async-done | bytes 262160 | tf_op jit(solution)/shard_map/reduce_scatter | solution.py:55
  233.0 1.1 multiply_reduce_fusion
  234.1 0.0 copy-done
  234.1 1.7 multiply_convert_fusion
  (8 shorter events, 0.1 us)
Async XLA Ops:
  6.5 73.2 %copy-start.1 = (f32[4]{0:T(128)S(1)}, f32[4]{0:T(128)}, u32[]{:S(2)}) copy-start(f32[4]{0:T(128)} %param.13) | copy-start | bytes 52
  6.5 57.7 %all-gather.14.cloned.1.call-start = ((), (), s32[]{:S(2)}) async-start(), calls=%async_computation.5 | async-start | bytes 6504960 | tf_op jit(solution)/shard_map/all_gather | solution.py:21
  10.6 67.3 %all-gather.12.cloned.1.call-start = ((), (), s32[]{:S(2)}) async-start(), calls=%async_computation.3 | async-start | bytes 1572864 | tf_op jit(solution)/shard_map/all_gather | solution.py:42
  33.4 99.4 %all-gather.8.cloned.1.call-start = ((), (), s32[]{:S(2)}) async-start(), calls=%async_computation.1 | async-start | bytes 8650752 | tf_op jit(solution)/shard_map/all_gather | solution.py:35
  75.9 116.7 %all-gather.10.cloned.1.call-start = ((), (), s32[]{:S(2)}) async-start(), calls=%async_computation.2 | async-start | bytes 8650752 | tf_op jit(solution)/shard_map/all_gather | solution.py:35
  76.5 156.5 %reduce-scatter.2.cloned.1.call-start = ((), (), s32[]{:S(2)}) async-start(), calls=%async_computation.4 | async-start | bytes 1310720 | tf_op jit(solution)/shard_map/reduce_scatter | solution.py:55
  192.6 41.5 %copy-start = (f32[1024]{0:T(1024)S(1)}, f32[1024]{0:T(1024)}, u32[]{:S(2)}) copy-start(f32[1024]{0:T(1024)} %param.15) | copy-start | bytes 12292
Sparse Core Ops, SparseCore 0:
  10.7 53.4 all-gather.13
  65.9 10.4 all-gather.11
  78.7 54.0 all-gather.7
  134.8 57.7 all-gather.9
  211.8 21.1 reduce-scatter.1
where the time goes:
time: 244 us; the launch traced here: 242 us
  waiting for transfers between devices  88.9 us (36%)
  blocking collectives  58.8 us (24%)
  matrix products  42 us (17%)
  other arithmetic  24.2 us (10%)
  local copies, waits for them, and re-layouts  15 us (6%)
  between operations  13.3 us (5%)
    all_gather x2, waiting for transfers between devices, taken_in(): lax.all_gather(a, axis, axis=dim, tiled=True)  49.6 us
    all_gather x1, blocking collectives, local(): gates_all = lax.all_gather(log_gate, SP, axis=0, tiled=True)  23.6 us
    all_gather x1, blocking collectives, all_blocks(): blocks = lax.all_gather(blocks, axes[k], axis=0, tiled=True)  21.8 us
    reduce_scatter x1, waiting for transfers between devices, summed_rows(): return lax.psum_scatter(whole, axis, scatter_dimension=0, tiled=True)  21.3 us
    dot_general x1, matrix products, update(): jnp.einsum('qhd,khd->hqk', queries, key_piece, preferred_element_type=jnp...  19.3 us
    reduce_sum x1, other arithmetic, update(): new_sum = run_sum * factor + jnp.sum(probs, axis=-1)  17.7 us
    dot_general x1, matrix products, update(): jnp.einsum('hqk,khd->hqd', probs, value_piece.astype(jnp.float32))  17.6 us
    all_gather x1, waiting for transfers between devices, one_gather(): lines, at, done = (lax.all_gather(ravelled, axis), 0, [])  17.4 us
  transfers between devices with their start and end apart: 5, of which 4 were waited for; matrix products, arithmetic and copies ran while one was open for 23% of the time, Pallas kernels for 0%

commit v1 on v0

v1 whole, which is shorter than its diff:
```python
import math

import jax
import jax.numpy as jnp
from jax import lax
from jax.experimental import pallas as pl
from jax.experimental.pallas import tpu as pltpu
from jax.sharding import Mesh
from jax.sharding import PartitionSpec as P

SP = ("z", "y", "c")
SP_TP = ("z", "y", "c", "x")
MESH = pl.DeviceIdType.MESH
F32 = jnp.float32
BF16 = jnp.bfloat16
LOG2E = math.log2(math.e)

RUN = 256
HD = 128
ROWS = 64


class Slots:
    def __init__(self):
        self.count = 0

    def take(self, n):
        at = self.count
        self.count += n
        return at


SEND = Slots()
RECV = Slots()


def ranges(**sizes):
    return {k: (SEND.take(n), RECV.take(n)) for k, n in sizes.items()}


SEM = ranges(
    xx=4,
    xz=12,
    w1=4,
    w2=12,
    w3=4,
    oy=4,
    oz=4,
    ox=12,
    op=4,
    kv=16,
    kp=16,
    gt=32,
    at=16,
)


def body(
    seq_len,
    x_ref,
    wq_ref,
    wk_ref,
    wv_ref,
    wg_ref,
    fb_ref,
    wo_ref,
    gain_ref,
    out_ref,
    xg,
    wp,
    wg,
    kv,
    gb,
    kbc,
    wo,
    att,
    a_in,
    qt,
    tb,
    acc,
    ms,
    ls,
    zt,
    ssem,
    rsem,
):
    z, y, c, x = (lax.axis_index(n) for n in ("z", "y", "c", "x"))

    def rem4(v):
        return lax.rem(v + 4, 4)

    xr, xl, xo = rem4(x + 1), rem4(x - 1), rem4(x + 2)
    yr, yl, yo = rem4(y + 1), rem4(y - 1), rem4(y + 2)
    zr, zl, zo = rem4(z + 1), rem4(z - 1), rem4(z + 2)
    other = 1 - c

    def copy(src, dst, kind, k, **to):
        s, r = SEM[kind]
        device = {"z": z, "y": y, "c": c, "x": x}
        device.update(to)
        return pltpu.make_async_remote_copy(
            src_ref=src,
            dst_ref=dst,
            send_sem=ssem.at[s + k],
            recv_sem=rsem.at[r + k],
            device_id=device,
            device_id_type=MESH,
        )

    def send(ref, kind, k, **to):
        copy(ref, ref, kind, k, **to).start()

    def got(ref, kind, k):
        copy(ref, ref, kind, k, c=other).wait_recv()

    def sent(ref, kind, k):
        copy(ref, ref, kind, k, c=other).wait_send()

    barrier = pltpu.get_barrier_semaphore()
    peers = []
    for dz in range(4):
        for dx in range(4):
            if dz or dx:
                peers.append(dict(z=rem4(z + dz), x=rem4(x + dx)))
    for dy in range(4):
        for dc in range(2):
            if dy or dc:
                peers.append(dict(y=rem4(y + dy), c=lax.rem(c + dc, 2)))
    for to in peers:
        device = {"z": z, "y": y, "c": c, "x": x}
        device.update(to)
        pl.semaphore_signal(barrier, inc=1, device_id=device, device_id_type=MESH)

    gate = wg_ref[...].astype(F32)
    for h in range(4):
        cols = slice(HD * h, HD * (h + 1))
        wp[h, :, 0:HD] = wq_ref[:, cols]
        wp[h, :, HD : 2 * HD] = wk_ref[:, cols]
        wp[h, :, 2 * HD : 3 * HD] = wv_ref[:, cols]
        wp[h, :, 3 * HD : 4 * HD] = jnp.broadcast_to(gate[:, h : h + 1], (32, HD)).astype(BF16)
    wg[z, y, c] = wp[z]
    xg[z, x] = x_ref[...]
    wo[x, z, y, c] = wo_ref[...]
    pl.semaphore_wait(barrier, len(peers))

    def w1(dz):
        return copy(wp.at[rem4(z + dz)], wg.at[z, y, c], "w1", dz, z=rem4(z + dz))

    def xpiece(zz, xx):
        return xg.at[zz, xx]

    def send_xz(k, xx):
        send(xpiece(z, xx), "xz", k, z=zr)
        send(xpiece(z, xx), "xz", 4 + k, z=zl)

    def wpiece(dz, yy):
        return wg.at[rem4(z - dz), yy, c]

    def send_w2(dz):
        send(wpiece(dz, y), "w2", dz, y=yr)
        send(wpiece(dz, y), "w2", 4 + dz, y=yl)

    for dz in (1, 3, 2):
        w1(dz).start()
    send(xpiece(z, x), "xx", 0, x=xr)
    send(xpiece(z, x), "xx", 1, x=xl)
    send_w2(0)
    send_xz(0, x)
    send(wo.at[x, z, y, c], "oy", 0, y=yr)
    send(wo.at[x, z, y, c], "oy", 1, y=yl)
    for dz in (1, 3, 2):
        got(wpiece(dz, y), "w1", dz)
        send_w2(dz)
    send(wg.at[:, y, c], "w3", 0, c=other)
    half = ROWS // 2
    got(xpiece(z, xl), "xx", 0)
    send(xg.at[z, xl, 0:half], "xx", 2, x=xr)
    send_xz(1, xl)
    got(xpiece(z, xr), "xx", 1)
    send(xg.at[z, xr, half:ROWS], "xx", 3, x=xl)
    send_xz(2, xr)
    for dz in (0, 3):
        got(wpiece(dz, yl), "w2", dz)
        send(wpiece(dz, yl), "w2", 8 + dz, y=yr)
    for dz in (1, 2):
        got(wpiece(dz, yr), "w2", 4 + dz)
        send(wpiece(dz, yr), "w2", 8 + dz, y=yl)
    for dz in (1, 2):
        got(wpiece(dz, yl), "w2", dz)
    send(wg.at[:, yl, c], "w3", 1, c=other)
    for dz in (0, 3):
        got(wpiece(dz, yr), "w2", 4 + dz)
    send(wg.at[:, yr, c], "w3", 2, c=other)
    got(xg.at[z, xo, 0:half], "xx", 2)
    got(xg.at[z, xo, half:ROWS], "xx", 3)
    send_xz(3, xo)
    got(wo.at[x, z, yl, c], "oy", 0)
    send(wo.at[x, z, yl, c, 0:16], "oy", 2, y=yr)
    got(wo.at[x, z, yr, c], "oy", 1)
    send(wo.at[x, z, yr, c, 16:32], "oy", 3, y=yl)
    for dz in (0, 3, 1, 2):
        got(wpiece(dz, yo), "w2", 8 + dz)
    send(wg.at[:, yo, c], "w3", 3, c=other)
    got(wo.at[x, z, yo, c, 0:16], "oy", 2)
    got(wo.at[x, z, yo, c, 16:32], "oy", 3)

    def oslab(xx, dz):
        return wo.at[xx, rem4(z - dz), :, c]

    def send_ox(dz):
        send(oslab(x, dz), "ox", dz, x=xr)
        send(oslab(x, dz), "ox", 4 + dz, x=xl)

    def forward_ox(dz):
        got(oslab(xl, dz), "ox", dz)
        got(oslab(xr, dz), "ox", 4 + dz)
        if dz in (0, 3):
            send(oslab(xl, dz), "ox", 8 + dz, x=xr)
        else:
            send(oslab(xr, dz), "ox", 8 + dz, x=xl)

    send(wo.at[x, z, :, c], "oz", 0, z=zr)
    send(wo.at[x, z, :, c], "oz", 1, z=zl)
    send_ox(0)
    got(wg.at[:, y, other], "w3", 0)
    got(wg.at[:, yl, other], "w3", 1)
    got(wg.at[:, yr, other], "w3", 2)
    got(wg.at[:, yo, other], "w3", 3)

    def level(i):
        first = jnp.where(i == 0, z, 0)
        second = jnp.where(i == 1, jnp.where(z == 0, 1, jnp.where(z == 2, 1, 0)), 0)
        third = jnp.where(i == 2, jnp.where(z == 0, 2, jnp.where(z == 1, 2, jnp.where(z == 2, 0, 1))), 0)
        last = jnp.where(i == 3, jnp.where(z == 3, 2, 3), 0)
        return first + second + third + last

    row = lax.broadcasted_iota(jnp.int32, (RUN, RUN), 0)
    col = lax.broadcasted_iota(jnp.int32, (RUN, RUN), 1)
    tri = jnp.where(row >= col, 1.0, 0.0).astype(BF16)
    offset = fb_ref[z]
    kappa = HD ** (-0.5) * LOG2E

    def gate_peers():
        k = 0
        for dy in range(4):
            for dc in range(2):
                if dy or dc:
                    yield k, rem4(y + dy), lax.rem(c + dc, 2), rem4(y - dy), lax.rem(c + dc, 2)
                k += 1

    def project(i):
        zb = level(i)
        rows = xg[zb].reshape(RUN, 1024)
        weights = wg[...].reshape(1024, 4 * HD)
        out = jnp.dot(rows, weights, preferred_element_type=F32)
        kv[zb, y, c, 0:RUN] = out[:, HD : 2 * HD].astype(BF16)
        vt = out[:, 2 * HD : 3 * HD].T.astype(BF16)
        kv[zb, y, c, RUN : RUN + HD] = vt[:, 0:HD]
        kv[zb, y, c, RUN + HD : RUN + 2 * HD] = vt[:, HD : 2 * HD]
        qt[zb] = out[:, 0:HD].T.astype(BF16)
        raw = out[:, 3 * HD : 4 * HD] + offset + math.log(seq_len)
        lg = jnp.minimum(raw, 0.0) - jnp.log1p(jnp.exp(-jnp.abs(raw)))
        hi = lg.astype(BF16)
        rest = lg - hi.astype(F32)
        mid = rest.astype(BF16)
        low = (rest - mid.astype(F32)).astype(BF16)
        sums = (
            jnp.dot(tri, hi, preferred_element_type=F32)
            + jnp.dot(tri, mid, preferred_element_type=F32)
            + jnp.dot(tri, low, preferred_element_type=F32)
        )
        gb[zb, y, c] = sums.T[0:8]
        for k, ty, tc, _, _ in gate_peers():
            send(gb.at[zb, y, c], "gt", i * 8 + k, y=ty, c=tc)
        send(kv.at[zb, y, c], "kv", i * 4, y=yr)
        send(kv.at[zb, y, c], "kv", i * 4 + 1, y=yl)
        send(kv.at[zb, y, c], "kp", i * 4, c=other)

    def relay(i):
        zb = level(i)
        got(kv.at[zb, yl, c], "kv", i * 4)
        send(kv.at[zb, yl, c, 0:RUN], "kv", i * 4 + 2, y=yr)
        send(kv.at[zb, yl, c], "kp", i * 4 + 1, c=other)
        got(kv.at[zb, yr, c], "kv", i * 4 + 1)
        send(kv.at[zb, yr, c, RUN : 2 * RUN], "kv", i * 4 + 3, y=yl)
        send(kv.at[zb, yr, c], "kp", i * 4 + 2, c=other)

    def gather_level(i):
        zb = level(i)
        got(kv.at[zb, yo, c, 0:RUN], "kv", i * 4 + 2)
        got(kv.at[zb, yo, c, RUN : 2 * RUN], "kv", i * 4 + 3)
        send(kv.at[zb, yo, c], "kp", i * 4 + 3, c=other)
        for k, _, _, sy, sc in gate_peers():
            got(gb.at[zb, sy, sc], "gt", i * 8 + k)
        base = jnp.zeros((8, RUN), F32)
        for yy in range(4):
            for cc in range(2):
                g = gb[zb, yy, cc]
                bias = (g + base) * (-LOG2E)
                kbc[zb, (2 * yy + cc) * RUN : (2 * yy + cc + 1) * RUN] = jnp.concatenate([bias] * 16, axis=0).T
                base = base + jnp.broadcast_to(g[:, RUN - 1 : RUN], (8, RUN))
        zt[zb] = base
        got(kv.at[zb, y, other], "kp", i * 4)
        got(kv.at[zb, yl, other], "kp", i * 4 + 1)
        got(kv.at[zb, yr, other], "kp", i * 4 + 2)
        got(kv.at[zb, yo, other], "kp", i * 4 + 3)

    chunk = 2 * RUN
    ahead = lax.broadcasted_iota(jnp.int32, (chunk, RUN), 0) - lax.broadcasted_iota(jnp.int32, (chunk, RUN), 1)

    def attend(i):
        def one(k, carry):
            late = k == 4
            za = jnp.where(late, level(3), k)
            zb = jnp.where(late, level(0), level(i))
            fits = jnp.where(late, i == 1, jnp.logical_or(i != 0, za != level(3)))

            @pl.when(jnp.logical_and(fits, za >= zb))
            def _():
                pair(za, zb)

            return carry

        def pair(za, zb):
            limit = jnp.where(za == zb, (2 * y + c) * RUN, 4 * chunk)
            top = jnp.full((1, RUN), -1e30, F32)
            for yy in range(4):
                keys = jnp.concatenate([kv[zb, yy, 0, 0:RUN], kv[zb, yy, 1, 0:RUN]], axis=0)
                s = jnp.dot(keys, qt[za], preferred_element_type=F32)
                b = kbc[zb, yy * chunk : (yy + 1) * chunk]
                t = s * kappa + jnp.concatenate([b, b], axis=1)
                t = jnp.where(ahead <= limit - yy * chunk, t, -1e30)
                tb[yy * chunk : (yy + 1) * chunk] = t
                top = jnp.maximum(top, jnp.max(t, axis=0, keepdims=True))
            total = jnp.zeros((1, RUN), F32)
            out = jnp.zeros((HD, RUN), F32)
            for yy in range(4):
                p = jnp.exp2(tb[yy * chunk : (yy + 1) * chunk] - top)
                total = total + jnp.sum(p, axis=0, keepdims=True)
                vt = jnp.concatenate(
                    [
                        kv[zb, yy, cc, RUN + k * HD : RUN + (k + 1) * HD]
                        for cc in range(2)
                        for k in range(2)
                    ],
                    axis=1,
                )
                out = out + jnp.dot(vt, p.astype(BF16), preferred_element_type=F32)
            acc[za, zb] = out
            ms[za, zb] = jnp.broadcast_to(top, (8, RUN))
            ls[za, zb] = jnp.broadcast_to(total, (8, RUN))

        lax.fori_loop(0, 5, one, 0)

    def step(i, carry):
        @pl.when(i == 1)
        def _():
            for k, xx in ((0, rem4(x)), (1, xl), (2, xr), (3, xo)):
                got(xpiece(zl, xx), "xz", k)
                if k in (0, 3):
                    send(xpiece(zl, xx), "xz", 8 + k, z=zr)
                got(xpiece(zr, xx), "xz", 4 + k)
                if k in (1, 2):
                    send(xpiece(zr, xx), "xz", 8 + k, z=zl)
            got(wo.at[x, zl, :, c], "oz", 0)
            send(wo.at[x, zl, 0:2, c], "oz", 2, z=zr)
            got(wo.at[x, zr, :, c], "oz", 1)
            send(wo.at[x, zr, 2:4, c], "oz", 3, z=zl)
            send_ox(1)
            send_ox(3)
            forward_ox(0)

        @pl.when(i == 2)
        def _():
            for k, xx in ((0, rem4(x)), (3, xo), (1, xl), (2, xr)):
                got(xpiece(zo, xx), "xz", 8 + k)

        @pl.when(i < 4)
        def _():
            project(i)

        @pl.when(i == 3)
        def _():
            got(wo.at[x, zo, 0:2, c], "oz", 2)
            got(wo.at[x, zo, 2:4, c], "oz", 3)
            send_ox(2)
            forward_ox(1)
            forward_ox(3)

        @pl.when(jnp.logical_and(i >= 1, i <= 4))
        def _():
            relay(i - 1)

        @pl.when(i == 4)
        def _():
            forward_ox(2)

        @pl.when(i >= 2)
        def _():
            gather_level(i - 2)
            attend(i - 2)

        return carry

    lax.fori_loop(0, 6, step, 0)

    def join(za, carry):
        shift = []
        base = jnp.zeros((8, RUN), F32)
        for zb in range(4):
            shift.append(base * (-LOG2E))
            base = base + zt[zb]
        top = jnp.full((8, RUN), -3e38, F32)
        for zb in range(4):
            top = jnp.where(za >= zb, jnp.maximum(top, ms[za, zb] + shift[zb]), top)
        total = jnp.zeros((8, RUN), F32)
        out = jnp.zeros((HD, RUN), F32)
        for zb in range(4):
            w = jnp.where(za >= zb, jnp.exp2(ms[za, zb] + shift[zb] - top), 0.0)
            total = total + jnp.where(za >= zb, w * ls[za, zb], 0.0)
            out = out + jnp.where(za >= zb, w[0:1] * acc[za, zb], 0.0)
        out = out / total[0:1]
        att[za] = out.T.astype(BF16).reshape(4, ROWS, HD)
        return carry

    lax.fori_loop(0, 4, join, 0)
    a_in[x, z] = att[z, x]

    def rows_to(dz, dx):
        tz, tx = rem4(z + dz), rem4(x + dx)
        return copy(att.at[tz, tx], a_in.at[x, z], "at", dz * 4 + dx, z=tz, x=tx)

    away = [(dz, dx) for dz in range(4) for dx in range(4) if dz or dx]
    for dz, dx in away:
        rows_to(dz, dx).start()
    for dz in (0, 3, 1, 2):
        part = oslab(xo, dz)
        got(part, "ox", 8 + dz)
    for k, xx in enumerate((x, xl, xr, xo)):
        send(wo.at[xx, :, :, c], "op", k, c=other)
    for k, xx in enumerate((x, xl, xr, xo)):
        got(wo.at[xx, :, :, other], "op", k)
    for dz, dx in away:
        got(a_in.at[rem4(x - dx), rem4(z - dz)], "at", dz * 4 + dx)

    summed = jnp.zeros((ROWS, 1024), F32)
    for xx in range(4):
        left = jnp.concatenate([a_in[xx, zz] for zz in range(4)], axis=1)
        right = wo[xx].reshape(1024, 512)
        summed = summed + lax.dot_general(left, right, (((1,), (1,)), ((), ())), preferred_element_type=F32)
    mean = jnp.mean(summed * summed, axis=-1, keepdims=True)
    out_ref[...] = (summed * lax.rsqrt(mean + 1e-06) * gain_ref[...]).astype(BF16)

    for dz in (1, 3, 2):
        w1(dz).wait_send()
    for k, xx in enumerate((x, x, xl, xr)):
        ref = xpiece(z, xx) if k < 2 else xg.at[z, xx, 0:half]
        sent(ref, "xx", k)
    for k in range(12):
        sent(xpiece(z, x), "xz", k)
        sent(wpiece(0, y), "w2", k)
        sent(oslab(x, 0), "ox", k)
    for k in range(4):
        sent(wg.at[:, y, c], "w3", k)
        sent(wo.at[x, z, y, c] if k < 2 else wo.at[x, z, y, c, 0:16], "oy", k)
        sent(wo.at[x, z, :, c] if k < 2 else wo.at[x, z, 0:2, c], "oz", k)
        sent(wo.at[x, :, :, c], "op", k)

    def drain(i, carry):
        for k in range(4):
            sent(kv.at[z, y, c] if k < 2 else kv.at[z, y, c, 0:RUN], "kv", i * 4 + k)
            sent(kv.at[z, y, c], "kp", i * 4 + k)
        for k in range(1, 8):
            sent(gb.at[z, y, c], "gt", i * 8 + k)
        return carry

    lax.fori_loop(0, 4, drain, 0)
    for dz, dx in away:
        rows_to(dz, dx).wait_send()


def local(tokens, query_weight, key_weight, value_weight, gate_weight, forget_bias, out_weight, out_gain):
    seq_len = tokens.shape[0] * lax.axis_size(SP_TP)
    vmem = pl.BlockSpec(memory_space=pltpu.VMEM)

    def kernel(*refs):
        body(seq_len, *refs)

    return pl.pallas_call(
        kernel,
        out_shape=jax.ShapeDtypeStruct(tokens.shape, BF16),
        in_specs=[vmem] * 5 + [pl.BlockSpec(memory_space=pltpu.SMEM)] + [vmem] * 2,
        out_specs=vmem,
        scratch_shapes=[
            pltpu.VMEM((4, 4, ROWS, 1024), BF16),
            pltpu.VMEM((4, 32, 512), BF16),
            pltpu.VMEM((4, 4, 2, 32, 512), BF16),
            pltpu.VMEM((4, 4, 2, 2 * RUN, HD), BF16),
            pltpu.VMEM((4, 4, 2, 8, RUN), F32),
            pltpu.VMEM((4, 8 * RUN, HD), F32),
            pltpu.VMEM((4, 4, 4, 2, 32, 512), BF16),
            pltpu.VMEM((4, 4, ROWS, HD), BF16),
            pltpu.VMEM((4, 4, ROWS, HD), BF16),
            pltpu.VMEM((4, HD, RUN), BF16),
            pltpu.VMEM((8 * RUN, RUN), F32),
            pltpu.VMEM((4, 4, HD, RUN), F32),
            pltpu.VMEM((4, 4, 8, RUN), F32),
            pltpu.VMEM((4, 4, 8, RUN), F32),
            pltpu.VMEM((4, 8, RUN), F32),
            pltpu.SemaphoreType.DMA((SEND.count,)),
            pltpu.SemaphoreType.DMA((RECV.count,)),
        ],
        compiler_params=pltpu.CompilerParams(
            collective_id=0, has_side_effects=True, vmem_limit_bytes=48 * 1024 * 1024
        ),
    )(
        tokens,
        query_weight,
        key_weight,
        value_weight,
        gate_weight,
        forget_bias,
        out_weight.T,
        out_gain.reshape(1, -1),
    )


def solution(mesh):
    torus = Mesh(mesh.devices.reshape(4, 4, 2, mesh.shape["tp"]), SP_TP)
    in_specs = (
        P(SP_TP, None),
        P(SP, "x"),
        P(SP, "x"),
        P(SP, "x"),
        P(SP, "x"),
        P("x"),
        P("x", SP),
        P(),
    )
    out_specs = P(SP_TP, None)
    return jax.shard_map(local, mesh=torus, in_specs=in_specs, out_specs=out_specs, check_vma=False)
```

time: 244 us -> 71.9 us (0.29)
  waiting for transfers between devices: 88.9 us -> 0 us
  Pallas kernels: 0 us -> 65.5 us
  blocking collectives: 58.8 us -> 0 us
  matrix products: 42 us -> 0 us
  other arithmetic: 24.2 us -> 0 us
  between operations: 13.3 us -> 0.02 us
  local copies, waits for them, and re-layouts: 15 us -> 5.96 us
    all_gather x4 -> x0, waiting for transfers between devices: 67 us -> none  [the longest x2 49.6 us: taken_in(): lax.all_gather(a, axis, axis=dim, tiled=True)]
    pallas_call x0 -> x1, Pallas kernels: none -> 65.5 us  [local(): pl.pallas_call(kernel, out_shape=jax.ShapeDtypeStruct(tokens.shape, BF16)...]
    all_gather x3 -> x0, blocking collectives: 58.8 us -> none  [the longest x1 23.6 us: local(): gates_all = lax.all_gather(log_gate, SP, axis=0, tiled=True)]
    dot_general x4 -> x0, matrix products: 42 us -> none  [the longest x1 19.3 us: update(): jnp.einsum('qhd,khd->hqk', queries, key_piece, preferred_element_type=jnp...]
    reduce_scatter x1 -> x0, waiting for transfers between devices: 21.3 us -> none  [summed_rows(): return lax.psum_scatter(whole, axis, scatter_dimension=0, tiled=True)]
    reduce_sum x2 -> x0, other arithmetic: 18.8 us -> none  [the longest x1 17.7 us: update(): new_sum = run_sum * factor + jnp.sum(probs, axis=-1)]
    another operation x4 -> x0, local copies, waits for them, and re-layouts: 2.91 us -> none  [in_order(): return jnp.moveaxis(blocks, 0, dim).reshape(shape)]
    unnamed x13 -> x18, local copies, waits for them, and re-layouts: 8.07 us -> 5.96 us
  transfers between devices with their start and end apart: 5 -> 0, of which waited for: 4 -> 0; matrix products, arithmetic and copies ran while one was open for 23% -> 0% of each run, Pallas kernels for 0% -> 0%
where the time goes in v1:
time: 71.9 us; the launch traced here: 71.4 us
  Pallas kernels  65.5 us (91%)
  local copies, waits for them, and re-layouts  5.96 us (8%)
    pallas_call x1, Pallas kernels, local(): pl.pallas_call(kernel, out_shape=jax.ShapeDtypeStruct(tokens.shape, BF16)...  65.5 us
    unnamed x18, local copies, waits for them, and re-layouts  5.96 us

profile of v1, /device:TPU:1, one launch (start us, length us, event | category | flops | bytes accessed | tf_op | source)
XLA Modules:
  0.0 71.4 jit_solution(2769400478047649981)
XLA Ops:
  0.0 0.0 copy-start.7
  0.0 0.7 copy-done.7
  0.7 0.0 copy-start.5
  0.7 0.0 copy-start.6
  0.7 0.1 copy.9.refs_4_
  0.8 0.6 copy-done.5
  1.4 0.0 copy-done.6
  1.4 0.0 copy-start
  1.4 0.9 %copy-done = bf16[64,1024]{1,0:T(8,128)(2,1)S(1)} copy-done((bf16[64,1024]{1,0:T(8,128)(2,1)S(1)}, bf16[64,1024]{1,0:T(8,128)(2,1)}, u32[]{:S(2)}) %copy-start) | copy-done | bytes 131096
  2.3 0.0 copy-start.1
  2.3 0.8 %copy-done.1 = bf16[32,512]{1,0:T(8,128)(2,1)S(1)} copy-done((bf16[32,512]{1,0:T(8,128)(2,1)S(1)}, bf16[32,512]{1,0:T(8,128)(2,1)}, u32[]{:S(2)}) %copy-start.1) | copy-done | bytes 32792
  3.0 0.0 copy-start.2
  3.0 0.8 %copy-done.2 = bf16[32,512]{1,0:T(8,128)(2,1)S(1)} copy-done((bf16[32,512]{1,0:T(8,128)(2,1)S(1)}, bf16[32,512]{1,0:T(8,128)(2,1)}, u32[]{:S(2)}) %copy-start.2) | copy-done | bytes 32792
  3.8 0.0 copy-start.3
  3.8 0.8 %copy-done.3 = bf16[32,512]{1,0:T(8,128)(2,1)S(1)} copy-done((bf16[32,512]{1,0:T(8,128)(2,1)S(1)}, bf16[32,512]{1,0:T(8,128)(2,1)}, u32[]{:S(2)}) %copy-start.3) | copy-done | bytes 32792
  4.6 0.0 copy-start.4
  4.6 0.8 %copy-done.4 = bf16[512,32]{0,1:T(8,128)(2,1)S(1)} copy-done((bf16[512,32]{0,1:T(8,128)(2,1)S(1)}, bf16[512,32]{0,1:T(8,128)(2,1)}, u32[]{:S(2)}) %copy-start.4) | copy-done | bytes 32792
  5.3 65.5 %shard_map.82 = bf16[64,1024]{1,0:T(8,128)(2,1)S(1)} custom-call(bf16[64,1024]{1,0:T(8,128)(2,1)S(1)} %copy-done, bf16[32,512]{1,0:T(8,128)(2,1)S(1)} %copy-done.1, bf16[32,512]{1,0:T(8,128)(2,1)S(1)} %copy-done.2, bf16[32,512]{1,0:T(8,128)(2,1)S(1)} %copy-done.3, bf16[32,4]{1,0:T(8,128)(2,1)S(1)} %copy.9.refs_4_, f32[4]{0:T(128)S(1)} %copy-done.6, ...), custom_call_target="tpu_custom_call" | custom-call | tf_op jit(solution)/shard_map/pallas_call | solution.py:489
  70.8 0.7 copy.11
Async XLA Ops:
  0.0 0.7 copy-start.7
  0.7 0.7 copy-start.5
  0.7 0.7 copy-start.6
  1.4 0.9 %copy-start = (bf16[64,1024]{1,0:T(8,128)(2,1)S(1)}, bf16[64,1024]{1,0:T(8,128)(2,1)}, u32[]{:S(2)}) copy-start(bf16[64,1024]{1,0:T(8,128)(2,1)} %refs_0_.1) | copy-start | bytes 393220
  2.3 0.8 %copy-start.1 = (bf16[32,512]{1,0:T(8,128)(2,1)S(1)}, bf16[32,512]{1,0:T(8,128)(2,1)}, u32[]{:S(2)}) copy-start(bf16[32,512]{1,0:T(8,128)(2,1)} %refs_1_.1) | copy-start | bytes 98308
  3.0 0.8 %copy-start.2 = (bf16[32,512]{1,0:T(8,128)(2,1)S(1)}, bf16[32,512]{1,0:T(8,128)(2,1)}, u32[]{:S(2)}) copy-start(bf16[32,512]{1,0:T(8,128)(2,1)} %refs_2_.1) | copy-start | bytes 98308
  3.8 0.8 %copy-start.3 = (bf16[32,512]{1,0:T(8,128)(2,1)S(1)}, bf16[32,512]{1,0:T(8,128)(2,1)}, u32[]{:S(2)}) copy-start(bf16[32,512]{1,0:T(8,128)(2,1)} %refs_3_.1) | copy-start | bytes 98308
  4.6 0.8 %copy-start.4 = (bf16[512,32]{0,1:T(8,128)(2,1)S(1)}, bf16[512,32]{0,1:T(8,128)(2,1)}, u32[]{:S(2)}) copy-start(bf16[512,32]{0,1:T(8,128)(2,1)} %param.14) | copy-start | bytes 98308

commit v2 on v1

--- a/solution.py
+++ b/solution.py
@@ -48,11 +48,14 @@
     oz=4,
     ox=12,
     op=4,
-    kv=16,
+    kv=24,
     kp=16,
     gt=32,
+    g1=4,
+    g2=8,
     at=16,
 )
+IN_TOKENS, IN_OUT, IN_GATE, IN_GAIN, IN_OWN, IN_HEADS, IN_COUNT = 0, 1, 2, 3, 4, 7, 19
 
 
 def body(
@@ -81,8 +84,13 @@
     ms,
     ls,
     zt,
+    gate_in,
+    gain_in,
+    grow,
+    gwb,
     ssem,
     rsem,
+    isem,
 ):
     z, y, c, x = (lax.axis_index(n) for n in ("z", "y", "c", "x"))
 
@@ -115,6 +123,24 @@
 
     def sent(ref, kind, k):
         copy(ref, ref, kind, k, c=other).wait_send()
+
+    ins = [
+        pltpu.make_async_copy(x_ref, xg.at[z, x], isem.at[IN_TOKENS]),
+        pltpu.make_async_copy(wg_ref, gate_in, isem.at[IN_GATE]),
+        pltpu.make_async_copy(wo_ref, wo.at[x, z, y, c], isem.at[IN_OUT]),
+        pltpu.make_async_copy(gain_ref, gain_in, isem.at[IN_GAIN]),
+    ]
+    own = pl.ds(pl.multiple_of(z * HD, HD), HD)
+    for j, ref in enumerate((wq_ref, wk_ref, wv_ref)):
+        to = slice(HD * j, HD * (j + 1))
+        ins.append(pltpu.make_async_copy(ref.at[:, own], wg.at[z, y, c, :, to], isem.at[IN_OWN + j]))
+        for h in range(4):
+            cols = slice(HD * h, HD * (h + 1))
+            ins.append(
+                pltpu.make_async_copy(ref.at[:, cols], wp.at[h, :, to], isem.at[IN_HEADS + 4 * j + h])
+            )
+    for one in ins:
+        one.start()
 
     barrier = pltpu.get_barrier_semaphore()
     peers = []
@@ -131,17 +157,19 @@
         device.update(to)
         pl.semaphore_signal(barrier, inc=1, device_id=device, device_id_type=MESH)
 
-    gate = wg_ref[...].astype(F32)
-    for h in range(4):
-        cols = slice(HD * h, HD * (h + 1))
-        wp[h, :, 0:HD] = wq_ref[:, cols]
-        wp[h, :, HD : 2 * HD] = wk_ref[:, cols]
-        wp[h, :, 2 * HD : 3 * HD] = wv_ref[:, cols]
-        wp[h, :, 3 * HD : 4 * HD] = jnp.broadcast_to(gate[:, h : h + 1], (32, HD)).astype(BF16)
-    wg[z, y, c] = wp[z]
-    xg[z, x] = x_ref[...]
-    wo[x, z, y, c] = wo_ref[...]
+    for one in ins:
+        one.wait()
+    gate = gate_in[...].astype(F32)
+    grow[z, y, c] = jnp.concatenate([gate[h : h + 1] for h in range(4)], axis=1)
     pl.semaphore_wait(barrier, len(peers))
+
+    def gate_peers():
+        k = 0
+        for dy in range(4):
+            for dc in range(2):
+                if dy or dc:
+                    yield k, rem4(y + dy), lax.rem(c + dc, 2), rem4(y - dy), lax.rem(c + dc, 2)
+                k += 1
 
     def w1(dz):
         return copy(wp.at[rem4(z + dz)], wg.at[z, y, c], "w1", dz, z=rem4(z + dz))
@@ -166,6 +194,8 @@
     send(xpiece(z, x), "xx", 1, x=xl)
     send_w2(0)
     send_xz(0, x)
+    for dz in (1, 3, 2):
+        send(grow.at[z, y, c], "g1", dz, z=rem4(z + dz))
     send(wo.at[x, z, y, c], "oy", 0, y=yr)
     send(wo.at[x, z, y, c], "oy", 1, y=yl)
     for dz in (1, 3, 2):
@@ -179,26 +209,31 @@
     got(xpiece(z, xr), "xx", 1)
     send(xg.at[z, xr, half:ROWS], "xx", 3, x=xl)
     send_xz(2, xr)
-    for dz in (0, 3):
-        got(wpiece(dz, yl), "w2", dz)
-        send(wpiece(dz, yl), "w2", 8 + dz, y=yr)
-    for dz in (1, 2):
-        got(wpiece(dz, yr), "w2", 4 + dz)
-        send(wpiece(dz, yr), "w2", 8 + dz, y=yl)
-    for dz in (1, 2):
+    for dz in (0, 1, 3, 2):
+        if dz in (0, 2):
+            got(wpiece(dz, yl), "w2", dz)
+            send(wpiece(dz, yl), "w2", 8 + dz, y=yr)
+        else:
+            got(wpiece(dz, yr), "w2", 4 + dz)
+            send(wpiece(dz, yr), "w2", 8 + dz, y=yl)
+    for dz in (1, 3):
         got(wpiece(dz, yl), "w2", dz)
     send(wg.at[:, yl, c], "w3", 1, c=other)
-    for dz in (0, 3):
+    for dz in (0, 2):
         got(wpiece(dz, yr), "w2", 4 + dz)
     send(wg.at[:, yr, c], "w3", 2, c=other)
     got(xg.at[z, xo, 0:half], "xx", 2)
     got(xg.at[z, xo, half:ROWS], "xx", 3)
     send_xz(3, xo)
+    for dz in (1, 3, 2):
+        got(grow.at[rem4(z - dz), y, c], "g1", dz)
+    for k, ty, tc, _, _ in gate_peers():
+        send(grow.at[:, y, c], "g2", k, y=ty, c=tc)
     got(wo.at[x, z, yl, c], "oy", 0)
     send(wo.at[x, z, yl, c, 0:16], "oy", 2, y=yr)
     got(wo.at[x, z, yr, c], "oy", 1)
     send(wo.at[x, z, yr, c, 16:32], "oy", 3, y=yl)
-    for dz in (0, 3, 1, 2):
+    for dz in (0, 1, 3, 2):
         got(wpiece(dz, yo), "w2", 8 + dz)
     send(wg.at[:, yo, c], "w3", 3, c=other)
     got(wo.at[x, z, yo, c, 0:16], "oy", 2)
@@ -236,70 +271,98 @@
 
     row = lax.broadcasted_iota(jnp.int32, (RUN, RUN), 0)
     col = lax.broadcasted_iota(jnp.int32, (RUN, RUN), 1)
-    tri = jnp.where(row >= col, 1.0, 0.0).astype(BF16)
+    tri = jnp.where(row <= col, 1.0, 0.0).astype(BF16)
     offset = fb_ref[z]
     kappa = HD ** (-0.5) * LOG2E
 
-    def gate_peers():
-        k = 0
-        for dy in range(4):
-            for dc in range(2):
-                if dy or dc:
-                    yield k, rem4(y + dy), lax.rem(c + dc, 2), rem4(y - dy), lax.rem(c + dc, 2)
-                k += 1
+    def across(a, b):
+        return lax.dot_general(a, b, (((1,), (1,)), ((), ())), preferred_element_type=F32)
+
+    place = lax.broadcasted_iota(jnp.int32, (16, RUN), 0)
+
+    def parts(rows):
+        hi = rows.astype(BF16).astype(F32)
+        mid = (rows - hi).astype(BF16).astype(F32)
+        low = rows - hi - mid
+        zero = jnp.zeros_like(rows)
+        picked = jnp.where(place == 0, hi, jnp.where(place == 1, mid, jnp.where(place == 2, low, zero)))
+        return picked.astype(BF16)
+
+    def gate_row():
+        for k, _, _, sy, sc in gate_peers():
+            got(grow.at[:, sy, sc], "g2", k)
+        table = grow[...].reshape(32, HD).astype(BF16)
+        deep = lax.broadcasted_iota(jnp.int32, (1024, 32), 0)
+        pick = jnp.where(deep // 32 == lax.broadcasted_iota(jnp.int32, (1024, 32), 1), 1.0, 0.0)
+        found = jnp.dot(pick.astype(BF16), table, preferred_element_type=F32)
+        deep = lax.broadcasted_iota(jnp.int32, (1024, HD), 0)
+        lane = lax.broadcasted_iota(jnp.int32, (1024, HD), 1)
+        found = jnp.where(lane == 32 * z + deep % 32, found, 0.0).astype(BF16)
+        gwb[...] = across(jnp.ones((16, HD), BF16), found).astype(BF16)
+
+    keys, vals = slice(0, RUN), slice(RUN, 2 * RUN)
 
     def project(i):
         zb = level(i)
         rows = xg[zb].reshape(RUN, 1024)
-        weights = wg[...].reshape(1024, 4 * HD)
+        weights = wg[...].reshape(1024, 3 * HD)
         out = jnp.dot(rows, weights, preferred_element_type=F32)
-        kv[zb, y, c, 0:RUN] = out[:, HD : 2 * HD].astype(BF16)
+        kv[zb, y, c, keys] = out[:, HD : 2 * HD].astype(BF16)
         vt = out[:, 2 * HD : 3 * HD].T.astype(BF16)
         kv[zb, y, c, RUN : RUN + HD] = vt[:, 0:HD]
         kv[zb, y, c, RUN + HD : RUN + 2 * HD] = vt[:, HD : 2 * HD]
-        qt[zb] = out[:, 0:HD].T.astype(BF16)
-        raw = out[:, 3 * HD : 4 * HD] + offset + math.log(seq_len)
+        send(kv.at[zb, y, c, keys], "kv", i * 6, y=yr)
+        send(kv.at[zb, y, c, vals], "kv", i * 6 + 1, y=yl)
+        send(kv.at[zb, y, c, vals], "kv", i * 6 + 2, y=yr)
+        send(kv.at[zb, y, c, keys], "kv", i * 6 + 3, y=yl)
+        send(kv.at[zb, y, c], "kp", i * 4, c=other)
+        q = (out[:, 0:HD].astype(BF16).astype(F32) * kappa).T
+        qt[zb, 0:HD] = q.astype(BF16)
+        qt[zb, HD : 2 * HD] = (q - q.astype(BF16).astype(F32)).astype(BF16)
+
+        @pl.when(i == 0)
+        def _():
+            gate_row()
+
+        raw = across(gwb[...], rows) + offset + math.log(seq_len)
         lg = jnp.minimum(raw, 0.0) - jnp.log1p(jnp.exp(-jnp.abs(raw)))
-        hi = lg.astype(BF16)
-        rest = lg - hi.astype(F32)
-        mid = rest.astype(BF16)
-        low = (rest - mid.astype(F32)).astype(BF16)
-        sums = (
-            jnp.dot(tri, hi, preferred_element_type=F32)
-            + jnp.dot(tri, mid, preferred_element_type=F32)
-            + jnp.dot(tri, low, preferred_element_type=F32)
-        )
-        gb[zb, y, c] = sums.T[0:8]
+        sums = jnp.dot(parts(lg), tri, preferred_element_type=F32)
+        gb[zb, y, c] = jnp.sum(sums, axis=0, keepdims=True)
         for k, ty, tc, _, _ in gate_peers():
             send(gb.at[zb, y, c], "gt", i * 8 + k, y=ty, c=tc)
-        send(kv.at[zb, y, c], "kv", i * 4, y=yr)
-        send(kv.at[zb, y, c], "kv", i * 4 + 1, y=yl)
-        send(kv.at[zb, y, c], "kp", i * 4, c=other)
 
     def relay(i):
         zb = level(i)
-        got(kv.at[zb, yl, c], "kv", i * 4)
-        send(kv.at[zb, yl, c, 0:RUN], "kv", i * 4 + 2, y=yr)
+        got(kv.at[zb, yl, c, keys], "kv", i * 6)
+        send(kv.at[zb, yl, c, keys], "kv", i * 6 + 4, y=yr)
+        got(kv.at[zb, yr, c, vals], "kv", i * 6 + 1)
+        send(kv.at[zb, yr, c, vals], "kv", i * 6 + 5, y=yl)
+        got(kv.at[zb, yl, c, vals], "kv", i * 6 + 2)
         send(kv.at[zb, yl, c], "kp", i * 4 + 1, c=other)
-        got(kv.at[zb, yr, c], "kv", i * 4 + 1)
-        send(kv.at[zb, yr, c, RUN : 2 * RUN], "kv", i * 4 + 3, y=yl)
+        got(kv.at[zb, yr, c, keys], "kv", i * 6 + 3)
         send(kv.at[zb, yr, c], "kp", i * 4 + 2, c=other)
 
     def gather_level(i):
         zb = level(i)
-        got(kv.at[zb, yo, c, 0:RUN], "kv", i * 4 + 2)
-        got(kv.at[zb, yo, c, RUN : 2 * RUN], "kv", i * 4 + 3)
+        got(kv.at[zb, yo, c, keys], "kv", i * 6 + 4)
+        got(kv.at[zb, yo, c, vals], "kv", i * 6 + 5)
         send(kv.at[zb, yo, c], "kp", i * 4 + 3, c=other)
         for k, _, _, sy, sc in gate_peers():
             got(gb.at[zb, sy, sc], "gt", i * 8 + k)
-        base = jnp.zeros((8, RUN), F32)
+        base = jnp.zeros((16, RUN), F32)
+        bias = []
         for yy in range(4):
             for cc in range(2):
-                g = gb[zb, yy, cc]
-                bias = (g + base) * (-LOG2E)
-                kbc[zb, (2 * yy + cc) * RUN : (2 * yy + cc + 1) * RUN] = jnp.concatenate([bias] * 16, axis=0).T
-                base = base + jnp.broadcast_to(g[:, RUN - 1 : RUN], (8, RUN))
-        zt[zb] = base
+                g = jnp.broadcast_to(gb[zb, yy, cc], (16, RUN))
+                bias.append(parts((g + base) * (-LOG2E)))
+                base = base + jnp.broadcast_to(g[:, RUN - 1 : RUN], (16, RUN))
+        kbc[zb] = lax.dot_general(
+            jnp.concatenate(bias, axis=1),
+            jnp.ones((16, HD), BF16),
+            (((0,), (0,)), ((), ())),
+            preferred_element_type=F32,
+        )
+        zt[zb] = base[0:8]
         got(kv.at[zb, y, other], "kp", i * 4)
         got(kv.at[zb, yl, other], "kp", i * 4 + 1)
         got(kv.at[zb, yr, other], "kp", i * 4 + 2)
@@ -315,40 +378,59 @@
             zb = jnp.where(late, level(0), level(i))
             fits = jnp.where(late, i == 1, jnp.logical_or(i != 0, za != level(3)))
 
-            @pl.when(jnp.logical_and(fits, za >= zb))
+            @pl.when(jnp.logical_and(fits, za > zb))
             def _():
                 pair(za, zb)
 
+            @pl.when(jnp.logical_and(fits, za == zb))
+            def _():
+                diagonal(zb)
+
             return carry
 
+        def logits(za, zb, yy):
+            k = jnp.concatenate([kv[zb, yy, 0, 0:RUN], kv[zb, yy, 1, 0:RUN]], axis=0)
+            t = jnp.dot(jnp.concatenate([k, k], axis=1), qt[za], preferred_element_type=F32)
+            b = kbc[zb, pl.ds(yy * chunk, chunk)]
+            return t + jnp.concatenate([b, b], axis=1)
+
+        def weighted(zb, yy, p):
+            vt = jnp.concatenate(
+                [kv[zb, yy, cc, RUN + k * HD : RUN + (k + 1) * HD] for cc in range(2) for k in range(2)],
+                axis=1,
+            )
+            vt = jnp.concatenate([vt, jnp.ones((16, chunk), BF16)], axis=0)
+            return jnp.dot(vt, p.astype(BF16), preferred_element_type=F32)
+
+        def keep(za, zb, out, top):
+            acc[za, zb] = out[0:HD]
+            ms[za, zb] = jnp.broadcast_to(top, (8, RUN))
+            ls[za, zb] = out[HD : HD + 8]
+
         def pair(za, zb):
-            limit = jnp.where(za == zb, (2 * y + c) * RUN, 4 * chunk)
             top = jnp.full((1, RUN), -1e30, F32)
             for yy in range(4):
-                keys = jnp.concatenate([kv[zb, yy, 0, 0:RUN], kv[zb, yy, 1, 0:RUN]], axis=0)
-                s = jnp.dot(keys, qt[za], preferred_element_type=F32)
-                b = kbc[zb, yy * chunk : (yy + 1) * chunk]
-                t = s * kappa + jnp.concatenate([b, b], axis=1)
-                t = jnp.where(ahead <= limit - yy * chunk, t, -1e30)
+                t = logits(za, zb, yy)
                 tb[yy * chunk : (yy + 1) * chunk] = t
                 top = jnp.maximum(top, jnp.max(t, axis=0, keepdims=True))
-            total = jnp.zeros((1, RUN), F32)
-            out = jnp.zeros((HD, RUN), F32)
+            out = jnp.zeros((HD + 16, RUN), F32)
             for yy in range(4):
-                p = jnp.exp2(tb[yy * chunk : (yy + 1) * chunk] - top)
-                total = total + jnp.sum(p, axis=0, keepdims=True)
-                vt = jnp.concatenate(
-                    [
-                        kv[zb, yy, cc, RUN + k * HD : RUN + (k + 1) * HD]
-                        for cc in range(2)
-                        for k in range(2)
-                    ],
-                    axis=1,
-                )
-                out = out + jnp.dot(vt, p.astype(BF16), preferred_element_type=F32)
-            acc[za, zb] = out
-            ms[za, zb] = jnp.broadcast_to(top, (8, RUN))
-            ls[za, zb] = jnp.broadcast_to(total, (8, RUN))
+                out = out + weighted(zb, yy, jnp.exp2(tb[yy * chunk : (yy + 1) * chunk] - top))
+            keep(za, zb, out, top)
+
+        def diagonal(zb):
+            def first(yy, top):
+                t = logits(zb, zb, yy)
+                t = jnp.where(ahead <= (2 * y + c) * RUN - yy * chunk, t, -1e30)
+                tb[pl.ds(yy * chunk, chunk)] = t
+                return jnp.maximum(top, jnp.max(t, axis=0, keepdims=True))
+
+            top = lax.fori_loop(0, y + 1, first, jnp.full((1, RUN), -1e30, F32))
+
+            def second(yy, out):
+                return out + weighted(zb, yy, jnp.exp2(tb[pl.ds(yy * chunk, chunk)] - top))
+
+            keep(zb, zb, lax.fori_loop(0, y + 1, second, jnp.zeros((HD + 16, RUN), F32)), top)
 
         lax.fori_loop(0, 5, one, 0)
 
@@ -404,7 +486,15 @@
 
     lax.fori_loop(0, 6, step, 0)
 
-    def join(za, carry):
+    def rows_to(n, tz, dx):
+        tx = rem4(x + dx)
+        return copy(att.at[tz, tx], a_in.at[x, z], "at", n * 4 + dx, z=tz, x=tx)
+
+    def send_rows(n, tz, dx):
+        rows_to(n, tz, dx).start()
+
+    def join(n, carry):
+        za = rem4(z + jnp.where(n == 0, 2, jnp.where(n == 1, 1, jnp.where(n == 2, 3, 0))))
         shift = []
         base = jnp.zeros((8, RUN), F32)
         for zb in range(4):
@@ -421,18 +511,22 @@
             out = out + jnp.where(za >= zb, w[0:1] * acc[za, zb], 0.0)
         out = out / total[0:1]
         att[za] = out.T.astype(BF16).reshape(4, ROWS, HD)
+        for dx in (2, 1, 3, 0):
+            tx = rem4(x + dx)
+            if dx:
+                send_rows(n, za, dx)
+            else:
+
+                @pl.when(n != 3)
+                def _():
+                    send_rows(n, za, 0)
+
         return carry
 
     lax.fori_loop(0, 4, join, 0)
     a_in[x, z] = att[z, x]
 
-    def rows_to(dz, dx):
-        tz, tx = rem4(z + dz), rem4(x + dx)
-        return copy(att.at[tz, tx], a_in.at[x, z], "at", dz * 4 + dx, z=tz, x=tx)
-
-    away = [(dz, dx) for dz in range(4) for dx in range(4) if dz or dx]
-    for dz, dx in away:
-        rows_to(dz, dx).start()
+    away = [(n, dz, dx) for n, dz in enumerate((2, 1, 3, 0)) for dx in range(4) if dz or dx]
     for dz in (0, 3, 1, 2):
         part = oslab(xo, dz)
         got(part, "ox", 8 + dz)
@@ -440,8 +534,8 @@
         send(wo.at[xx, :, :, c], "op", k, c=other)
     for k, xx in enumerate((x, xl, xr, xo)):
         got(wo.at[xx, :, :, other], "op", k)
-    for dz, dx in away:
-        got(a_in.at[rem4(x - dx), rem4(z - dz)], "at", dz * 4 + dx)
+    for n, dz, dx in away:
+        got(a_in.at[rem4(x - dx), rem4(z - dz)], "at", n * 4 + dx)
 
     summed = jnp.zeros((ROWS, 1024), F32)
     for xx in range(4):
@@ -449,10 +543,13 @@
         right = wo[xx].reshape(1024, 512)
         summed = summed + lax.dot_general(left, right, (((1,), (1,)), ((), ())), preferred_element_type=F32)
     mean = jnp.mean(summed * summed, axis=-1, keepdims=True)
-    out_ref[...] = (summed * lax.rsqrt(mean + 1e-06) * gain_ref[...]).astype(BF16)
+    out_ref[...] = (summed * lax.rsqrt(mean + 1e-06) * gain_in[...]).astype(BF16)
 
     for dz in (1, 3, 2):
         w1(dz).wait_send()
+        sent(grow.at[z, y, c], "g1", dz)
+    for k in range(1, 8):
+        sent(grow.at[:, y, c], "g2", k)
     for k, xx in enumerate((x, x, xl, xr)):
         ref = xpiece(z, xx) if k < 2 else xg.at[z, xx, 0:half]
         sent(ref, "xx", k)
@@ -468,20 +565,22 @@
 
     def drain(i, carry):
         for k in range(4):
-            sent(kv.at[z, y, c] if k < 2 else kv.at[z, y, c, 0:RUN], "kv", i * 4 + k)
             sent(kv.at[z, y, c], "kp", i * 4 + k)
+        for k in range(6):
+            sent(kv.at[z, y, c, keys], "kv", i * 6 + k)
         for k in range(1, 8):
             sent(gb.at[z, y, c], "gt", i * 8 + k)
         return carry
 
     lax.fori_loop(0, 4, drain, 0)
-    for dz, dx in away:
-        rows_to(dz, dx).wait_send()
+    for n, dz, dx in away:
+        rows_to(n, rem4(z + dz), dx).wait_send()
 
 
 def local(tokens, query_weight, key_weight, value_weight, gate_weight, forget_bias, out_weight, out_gain):
     seq_len = tokens.shape[0] * lax.axis_size(SP_TP)
     vmem = pl.BlockSpec(memory_space=pltpu.VMEM)
+    hbm = pl.BlockSpec(memory_space=pltpu.HBM)
 
     def kernel(*refs):
         body(seq_len, *refs)
@@ -489,36 +588,41 @@
     return pl.pallas_call(
         kernel,
         out_shape=jax.ShapeDtypeStruct(tokens.shape, BF16),
-        in_specs=[vmem] * 5 + [pl.BlockSpec(memory_space=pltpu.SMEM)] + [vmem] * 2,
+        in_specs=[hbm] * 5 + [pl.BlockSpec(memory_space=pltpu.SMEM)] + [hbm] * 2,
         out_specs=vmem,
         scratch_shapes=[
             pltpu.VMEM((4, 4, ROWS, 1024), BF16),
-            pltpu.VMEM((4, 32, 512), BF16),
-            pltpu.VMEM((4, 4, 2, 32, 512), BF16),
+            pltpu.VMEM((4, 32, 3 * HD), BF16),
+            pltpu.VMEM((4, 4, 2, 32, 3 * HD), BF16),
             pltpu.VMEM((4, 4, 2, 2 * RUN, HD), BF16),
-            pltpu.VMEM((4, 4, 2, 8, RUN), F32),
+            pltpu.VMEM((4, 4, 2, 1, RUN), F32),
             pltpu.VMEM((4, 8 * RUN, HD), F32),
             pltpu.VMEM((4, 4, 4, 2, 32, 512), BF16),
             pltpu.VMEM((4, 4, ROWS, HD), BF16),
             pltpu.VMEM((4, 4, ROWS, HD), BF16),
-            pltpu.VMEM((4, HD, RUN), BF16),
+            pltpu.VMEM((4, 2 * HD, RUN), BF16),
             pltpu.VMEM((8 * RUN, RUN), F32),
             pltpu.VMEM((4, 4, HD, RUN), F32),
             pltpu.VMEM((4, 4, 8, RUN), F32),
             pltpu.VMEM((4, 4, 8, RUN), F32),
             pltpu.VMEM((4, 8, RUN), F32),
+            pltpu.VMEM((4, 32), BF16),
+            pltpu.VMEM((1, 1024), F32),
+            pltpu.VMEM((4, 4, 2, 1, HD), F32),
+            pltpu.VMEM((16, 1024), BF16),
             pltpu.SemaphoreType.DMA((SEND.count,)),
             pltpu.SemaphoreType.DMA((RECV.count,)),
+            pltpu.SemaphoreType.DMA((IN_COUNT,)),
         ],
         compiler_params=pltpu.CompilerParams(
-            collective_id=0, has_side_effects=True, vmem_limit_bytes=48 * 1024 * 1024
+            collective_id=0, has_side_effects=True, vmem_limit_bytes=67043328
         ),
     )(
         tokens,
         query_weight,
         key_weight,
         value_weight,
-        gate_weight,
+        gate_weight.T,
         forget_bias,
         out_weight.T,
         out_gain.reshape(1, -1),

time: 71.9 us -> 65.4 us (0.910)
  local copies, waits for them, and re-layouts: 5.96 us -> 1.57 us
  Pallas kernels: 65.5 us -> 63.2 us
    unnamed x18 -> x1, local copies, waits for them, and re-layouts: 5.96 us -> 1.57 us
    pallas_call x1, Pallas kernels: 65.5 us -> 63.2 us  [local(): pl.pallas_call(kernel, out_shape=jax.ShapeDtypeStruct(tokens.shape, BF16)...]
where the time goes in v2:
time: 65.4 us; the launch traced here: 64.8 us
  Pallas kernels  63.2 us (97%)
  local copies, waits for them, and re-layouts  1.57 us (2%)
    pallas_call x1, Pallas kernels, local(): pl.pallas_call(kernel, out_shape=jax.ShapeDtypeStruct(tokens.shape, BF16)...  63.2 us
    unnamed x1, local copies, waits for them, and re-layouts  1.57 us

profile of v2, /device:TPU:1, one launch (start us, length us, event | category | flops | bytes accessed | tf_op | source)
XLA Modules:
  0.0 64.8 jit_solution(15865026824829410223)
XLA Ops:
  0.0 63.2 %shard_map.82 = bf16[64,1024]{1,0:T(8,128)(2,1)} custom-call(bf16[64,1024]{1,0:T(8,128)(2,1)} %refs_0_.1, bf16[32,512]{1,0:T(8,128)(2,1)} %refs_1_.1, bf16[32,512]{1,0:T(8,128)(2,1)} %refs_2_.1, bf16[32,512]{1,0:T(8,128)(2,1)} %refs_3_.1, bf16[4,32]{1,0:T(4,128)(2,1)} %bitcast.5, f32[4]{0:T(128)} %refs_5_.1, bf16[32,512]{1,0:T(8,128)(2,1)} %bitcast.3, ...), custom_call_target="tpu_custom_call" | custom-call | tf_op jit(solution)/shard_map/pallas_call | solution.py:588
  63.2 1.6 %copy.10 = bf16[64,1024]{1,0:T(8,128)(2,1)} copy(bf16[64,1024]{1,0:T(8,128)(2,1)} %shard_map.82) | data formatting | bytes 262144

commit v3 on v2

--- a/solution.py
+++ b/solution.py
@@ -257,6 +257,17 @@
     send(wo.at[x, z, :, c], "oz", 0, z=zr)
     send(wo.at[x, z, :, c], "oz", 1, z=zl)
     send_ox(0)
+
+    def relay_xz(k, xx):
+        got(xpiece(zl, xx), "xz", k)
+        if k in (0, 3):
+            send(xpiece(zl, xx), "xz", 8 + k, z=zr)
+        got(xpiece(zr, xx), "xz", 4 + k)
+        if k in (1, 2):
+            send(xpiece(zr, xx), "xz", 8 + k, z=zl)
+
+    for k, xx in ((0, x), (1, xl), (2, xr)):
+        relay_xz(k, xx)
     got(wg.at[:, y, other], "w3", 0)
     got(wg.at[:, yl, other], "w3", 1)
     got(wg.at[:, yr, other], "w3", 2)
@@ -437,13 +448,7 @@
     def step(i, carry):
         @pl.when(i == 1)
         def _():
-            for k, xx in ((0, rem4(x)), (1, xl), (2, xr), (3, xo)):
-                got(xpiece(zl, xx), "xz", k)
-                if k in (0, 3):
-                    send(xpiece(zl, xx), "xz", 8 + k, z=zr)
-                got(xpiece(zr, xx), "xz", 4 + k)
-                if k in (1, 2):
-                    send(xpiece(zr, xx), "xz", 8 + k, z=zl)
+            relay_xz(3, xo)
             got(wo.at[x, zl, :, c], "oz", 0)
             send(wo.at[x, zl, 0:2, c], "oz", 2, z=zr)
             got(wo.at[x, zr, :, c], "oz", 1)

time: 65.4 us -> 65.3 us (level)
  no operation moved by 1% of the time
where the time goes in v3:
time: 65.3 us; the launch traced here: 65 us
  Pallas kernels  63.4 us (97%)
  local copies, waits for them, and re-layouts  1.57 us (2%)
    pallas_call x1, Pallas kernels, local(): pl.pallas_call(kernel, out_shape=jax.ShapeDtypeStruct(tokens.shape, BF16)...  63.4 us
    unnamed x1, local copies, waits for them, and re-layouts  1.57 us

profile of v3, /device:TPU:1, one launch (start us, length us, event | category | flops | bytes accessed | tf_op | source)
XLA Modules:
  0.0 65.0 jit_solution(10258465107993576513)
XLA Ops:
  0.0 63.4 %shard_map.82 = bf16[64,1024]{1,0:T(8,128)(2,1)} custom-call(bf16[64,1024]{1,0:T(8,128)(2,1)} %refs_0_.1, bf16[32,512]{1,0:T(8,128)(2,1)} %refs_1_.1, bf16[32,512]{1,0:T(8,128)(2,1)} %refs_2_.1, bf16[32,512]{1,0:T(8,128)(2,1)} %refs_3_.1, bf16[4,32]{1,0:T(4,128)(2,1)} %bitcast.5, f32[4]{0:T(128)} %refs_5_.1, bf16[32,512]{1,0:T(8,128)(2,1)} %bitcast.3, ...), custom_call_target="tpu_custom_call" | custom-call | tf_op jit(solution)/shard_map/pallas_call | solution.py:593
  63.4 1.6 %copy.10 = bf16[64,1024]{1,0:T(8,128)(2,1)} copy(bf16[64,1024]{1,0:T(8,128)(2,1)} %shard_map.82) | data formatting | bytes 262144
